TPU v7x, 32 devices: a whole 2x2x4 slice. The times are simulated.
32 devices in a mesh: fs: 8 (over z, y), tp: 4 (over x, core).
Axes of the slice: x: 2, y: 2, z: 4, core: 2. Of those that a mesh axis runs over, the one named last changes fastest.
Arguments:
- x_saved: bfloat16 [16384, 2048], P('fs'), may hold values from -6 to 6
- h_saved: bfloat16 [16384, 1024], P('fs', 'tp'), may hold values from -6 to 6
- key_cot: bfloat16 [16384, 1024], P('fs', 'tp'), may hold values from -6 to 6
- value_cot: bfloat16 [16384, 1024], P('fs', 'tp'), may hold values from -6 to 6
- out_cot: bfloat16 [16384, 2048], P('fs'), may hold values from -6 to 6
- w_key: float32 [2048, 1024], P('fs', 'tp'), may hold values from -0.125 to 0.125
- w_value: float32 [2048, 1024], P('fs', 'tp'), may hold values from -0.125 to 0.125
- w_out: float32 [1024, 2048], P('tp', 'fs'), may hold values from -0.1875 to 0.1875
- p_key: bfloat16 [2048, 256], P('fs'), may hold values from -1 to 1, as said below
- p_value: bfloat16 [2048, 256], P('fs'), may hold values from -1 to 1, as said below
- p_out: bfloat16 [2048, 256], P('fs'), may hold values from -1 to 1, as said below
- m_key: float32 [2, 256, 1024], P(None, 'fs', 'tp'), may hold values from -1.5 to 1.5, as said below
- m_value: float32 [2, 256, 1024], P(None, 'fs', 'tp'), may hold values from -1.5 to 1.5, as said below
- m_out: float32 [2, 256, 1024], P(None, 'fs', 'tp'), may hold values from -1.5 to 1.5, as said below
Outputs:
- step_key: float32 [2048, 1024], P('fs', 'tp')
- step_value: float32 [2048, 1024], P('fs', 'tp')
- step_out: float32 [1024, 2048], P('tp', 'fs')
- copy_key: bfloat16 [2048, 1024], P(None, 'tp')
- copy_value: bfloat16 [2048, 1024], P(None, 'tp')
- copy_out: bfloat16 [1024, 2048], P('tp')
- new_m_key: float32 [2, 256, 1024], P(None, 'fs', 'tp')
- new_m_value: float32 [2, 256, 1024], P(None, 'fs', 'tp')
- new_m_out: float32 [2, 256, 1024], P(None, 'fs', 'tp')
Inputs may be any that keep to these rules, and one draw needn't show every extreme that they name: `p_key`: factor entries are real-valued, dense and of full rank. `p_value`: factor entries are real-valued, dense and of full rank. `p_out`: factor entries are real-valued, dense and of full rank. `m_key`: plane 1 (second moments) lies in 0.05 to 1. `m_value`: plane 1 (second moments) lies in 0.05 to 1. `m_out`: plane 1 (second moments) lies in 0.05 to 1.
All inputs are finite; a program needn't handle non-finite values.
Results may differ from a plain program's by a relative error of at most 0.0085.
Values may be sent and summed in bfloat16 or wider, within the bound.
A program may use at most 128 MiB of HBM per device.

v0:
```python
import jax
import jax.numpy as jnp
from jax import lax
from jax.sharding import PartitionSpec as P

beta_one = 0.9
beta_two = 0.9
learn_rate = 0.01


def project_rows(factors, grads, local_width):
    high_part = grads.astype(jnp.bfloat16)
    low_part = (grads - high_part.astype(jnp.float32)).astype(jnp.bfloat16)
    outputs = []
    for member in range(3):
        lower = member * local_width
        upper = (member + 1) * local_width
        factor_t = factors[member].T
        first_term = jnp.dot(
            factor_t, high_part[:, lower:upper], preferred_element_type=jnp.float32
        )
        second_term = jnp.dot(
            factor_t, low_part[:, lower:upper], preferred_element_type=jnp.float32
        )
        outputs.append(first_term + second_term)
    return jnp.concatenate(outputs, axis=1)


def body(
    x_saved,
    h_saved,
    key_cot,
    value_cot,
    out_cot,
    w_key,
    w_value,
    w_out,
    p_key,
    p_value,
    p_out,
    m_key,
    m_value,
    m_out,
):
    local_width = key_cot.shape[1]
    x_cols = x_saved.T
    y_cols = out_cot.T
    grad_k = jnp.dot(x_cols, key_cot, preferred_element_type=jnp.float32)
    grad_v = jnp.dot(x_cols, value_cot, preferred_element_type=jnp.float32)
    grad_o = jnp.dot(y_cols, h_saved, preferred_element_type=jnp.float32)
    whole_grad = jnp.concatenate([grad_k, grad_v, grad_o], axis=1)
    partial_value = project_rows(
        (
            lax.all_gather(p_key, "fs", axis=0, tiled=True),
            lax.all_gather(p_value, "fs", axis=0, tiled=True),
            lax.all_gather(p_out, "fs", axis=0, tiled=True),
        ),
        whole_grad,
        local_width,
    )
    projected = lax.psum_scatter(partial_value, "fs", scatter_dimension=0, tiled=True)
    total = lax.psum(jnp.sum(projected * projected), ("fs", "tp"))
    entries = projected.size * lax.axis_size("fs") * lax.axis_size("tp")
    normed = projected / jnp.sqrt(total / entries + 1e-06)
    moments = jnp.concatenate([m_key, m_value, m_out], axis=2)
    moment_one = beta_one * moments[0] + (1 - beta_one) * normed
    moment_two = beta_two * moments[1] + (1 - beta_two) * normed * normed
    direction = (moment_one / jnp.sqrt(moment_two)).astype(jnp.bfloat16)
    gathered = lax.all_gather(direction, "fs", axis=0, tiled=True)
    step_key = jnp.dot(p_key, gathered[:, :local_width], preferred_element_type=jnp.float32)
    step_value = jnp.dot(
        p_value, gathered[:, local_width : 2 * local_width], preferred_element_type=jnp.float32
    )
    step_out = jnp.dot(p_out, gathered[:, 2 * local_width :], preferred_element_type=jnp.float32).T
    fresh_key = (w_key - learn_rate * step_key).astype(jnp.bfloat16)
    fresh_value = (w_value - learn_rate * step_value).astype(jnp.bfloat16)
    fresh_out = (w_out - learn_rate * step_out).astype(jnp.bfloat16)
    copy_key, copy_value, copy_out = (
        lax.all_gather(fresh_key, "fs", axis=0, tiled=True),
        lax.all_gather(fresh_value, "fs", axis=0, tiled=True),
        lax.all_gather(fresh_out, "fs", axis=1, tiled=True),
    )
    stacked = jnp.stack([moment_one, moment_two])
    new_m_key = stacked[:, :, :local_width]
    new_m_value = stacked[:, :, local_width : 2 * local_width]
    new_m_out = stacked[:, :, 2 * local_width :]
    return (
        step_key,
        step_value,
        step_out,
        copy_key,
        copy_value,
        copy_out,
        new_m_key,
        new_m_value,
        new_m_out,
    )


def solution(mesh):
    in_specs = (
        P("fs", None),
        P("fs", "tp"),
        P("fs", "tp"),
        P("fs", "tp"),
        P("fs", None),
        P("fs", "tp"),
        P("fs", "tp"),
        P("tp", "fs"),
        P("fs", None),
        P("fs", None),
        P("fs", None),
        P(None, "fs", "tp"),
        P(None, "fs", "tp"),
        P(None, "fs", "tp"),
    )
    out_specs = (
        P("fs", "tp"),
        P("fs", "tp"),
        P("tp", "fs"),
        P(None, "tp"),
        P(None, "tp"),
        P("tp", None),
        P(None, "fs", "tp"),
        P(None, "fs", "tp"),
        P(None, "fs", "tp"),
    )
    return jax.shard_map(body, mesh=mesh, in_specs=in_specs, out_specs=out_specs, check_vma=False)
```

profile of v0, /device:TPU:0, one launch (start us, length us, event | category | flops | bytes accessed | tf_op | source)
XLA Modules:
  0.0 409.5 jit_solution(15238596800766914783)
XLA Ops:
  7.2 0.0 copy-start
  7.2 0.0 all-gather.7.cloned.1.call-start
  7.2 0.7 all-gather.7.cloned.1.call-update
  7.9 0.0 all-gather.9.cloned.1.call-start
  8.0 0.7 all-gather.9.cloned.1.call-update
  8.7 0.0 all-gather.11.cloned.1.call-start
  8.7 0.7 all-gather.11.cloned.1.call-update
  9.4 0.0 reduce-scatter.4.cloned.1.call-start
  9.5 0.0 slice-start
  9.5 5.9 %fusion.23 = f32[2048,256]{0,1:T(8,128)S(1)} fusion(bf16[2048,2048]{1,0:T(8,128)(2,1)} %param.14, bf16[2048,256]{1,0:T(8,128)(2,1)S(1)} %copy-done), kind=kOutput, calls=%fused_computation.47 | convolution fusion | flops 2147483648 | bytes 11534336 | tf_op jit(solution)/shard_map/dot_general | solution.py:48
  15.4 0.0 slice-start.1
  15.4 5.9 %fusion.24 = f32[2048,256]{0,1:T(8,128)S(1)} fusion(bf16[2048,2048]{1,0:T(8,128)(2,1)} %param.14, bf16[2048,256]{1,0:T(8,128)(2,1)S(1)} %copy-done.6), kind=kOutput, calls=%fused_computation.48 | convolution fusion | flops 2147483648 | bytes 11534336 | tf_op jit(solution)/shard_map/dot_general | solution.py:49
  21.4 2.4 fusion.25
  23.8 2.0 fusion
  25.8 2.1 subtract_convert_fusion
  27.8 25.3 %all-gather.7.cloned.1.call-done = bf16[2048,256]{1,0:T(8,128)(2,1)} async-done(((bf16[256,256]{1,0:T(8,128)(2,1)}), bf16[2048,256]{1,0:T(8,128)(2,1)}) %all-gather.7.cloned.1.call-update) | async-done | bytes 1048592 | tf_op jit(solution)/shard_map/all_gather | solution.py:54
  53.2 2.1 fusion.11
  55.2 39.1 %all-gather.9.cloned.1.call-done = bf16[2048,256]{1,0:T(8,128)(2,1)} async-done(((bf16[256,256]{1,0:T(8,128)(2,1)}), bf16[2048,256]{1,0:T(8,128)(2,1)}) %all-gather.9.cloned.1.call-update) | async-done | bytes 1048592 | tf_op jit(solution)/shard_map/all_gather | solution.py:55
  94.3 2.1 fusion.8
  96.4 1.7 fusion.3
  98.1 1.7 fusion.2
  99.7 35.7 %all-gather.11.cloned.1.call-done = bf16[2048,256]{1,0:T(8,128)(2,1)} async-done(((bf16[256,256]{1,0:T(8,128)(2,1)}), bf16[2048,256]{1,0:T(8,128)(2,1)}) %all-gather.11.cloned.1.call-update) | async-done | bytes 1048592 | tf_op jit(solution)/shard_map/all_gather | solution.py:56
  135.5 2.0 fusion.5
  137.4 0.0 copy-start.3
  137.5 2.0 fusion.1
  139.5 0.0 copy-start.2
  139.5 0.1 pad_maximum_fusion.1
  139.6 1.1 copy.52
  140.7 0.0 reduce-scatter.4.cloned.1.call-update
  140.8 0.0 all-gather.17.cloned.1.call-start
  140.9 0.2 copy.54
  141.1 0.2 copy.55
  141.2 61.6 %reduce-scatter.4.cloned.1.call-done = f32[32,768]{1,0:T(8,128)} async-done(((f32[256,768]{1,0:T(8,128)}), f32[32,768]{1,0:T(8,128)}) %reduce-scatter.4.cloned.1.call-update) | async-done | bytes 98320
  202.9 1.1 copy.53
  203.9 0.7 multiply_reduce_fusion
  204.7 0.1 copy.44
  204.8 40.2 %psum.7 = f32[]{:T(128)} all-reduce(f32[]{:T(128)} %multiply_reduce_fusion), channel_id=1, replica_groups=mesh['fs'=8,'tp'=4] {'fs','tp'}, use_global_device_ids=true, to_apply=%region_2.0 | all-reduce | flops 1 | bytes 8 | tf_op jit(solution)/shard_map/psum | solution.py:62
  245.6 0.1 fusion.21
  245.8 0.1 copy.40
  245.9 31.0 %all_gather.24 = bf16[256,768]{1,0:T(8,128)(2,1)S(1)} all-gather(bf16[32,768]{1,0:T(8,128)(2,1)S(1)} %copy.40), channel_id=1, replica_groups=mesh['fs'=8,'tp'=4] {'fs'}, dimensions={0}, use_global_device_ids=true | all-gather | bytes 442368 | tf_op jit(solution)/shard_map/all_gather | solution.py:69
  276.9 1.1 fusion.14
  278.0 0.0 copy-start.1
  278.0 0.1 copy.43
  278.2 0.7 subtract_convert_fusion.1
  278.9 0.0 all-gather.17.cloned.1.call-update
  278.9 0.0 all-gather.15.cloned.1.call-start
  278.9 1.1 copy.42
  280.0 1.8 subtract_convert_fusion.2
  281.8 0.0 all-gather.15.cloned.1.call-update
  281.8 0.0 all-gather.13.cloned.1.call-start
  281.9 1.1 copy.41
  283.0 1.8 subtract_convert_fusion.3
  284.8 0.0 all-gather.13.cloned.1.call-update
  284.8 0.1 copy.45
  284.9 0.1 copy.46
  285.1 0.8 copy.48
  285.9 0.8 copy.47
  286.7 0.7 pad_maximum_fusion.2
  287.4 31.3 %all-gather.17.cloned.1.call-done = bf16[256,2048]{0,1:T(8,128)(2,1)} async-done(((bf16[256,256]{0,1:T(8,128)(2,1)}), bf16[256,2048]{0,1:T(8,128)(2,1)}) %all-gather.17.cloned.1.call-update) | async-done | bytes 1048592 | tf_op jit(solution)/shard_map/all_gather | solution.py:81
  318.8 2.3 copy.51
  321.0 38.4 %all-gather.15.cloned.1.call-done = bf16[2048,256]{0,1:T(8,128)(2,1)} async-done(((bf16[256,256]{0,1:T(8,128)(2,1)}), bf16[2048,256]{0,1:T(8,128)(2,1)}) %all-gather.15.cloned.1.call-update) | async-done | bytes 1048592 | tf_op jit(solution)/shard_map/all_gather | solution.py:80
  359.4 2.3 copy.50
  361.6 38.8 %all-gather.13.cloned.1.call-done = bf16[2048,256]{0,1:T(8,128)(2,1)} async-done(((bf16[256,256]{0,1:T(8,128)(2,1)}), bf16[2048,256]{0,1:T(8,128)(2,1)}) %all-gather.13.cloned.1.call-update) | async-done | bytes 1048592 | tf_op jit(solution)/shard_map/all_gather | solution.py:79
  400.4 2.3 copy.49
  (23 shorter events, 0.1 us)
Async XLA Ops:
  7.2 2.3 copy-start
  7.2 46.0 %all-gather.7.cloned.1.call-start = ((), (), s32[]{:S(2)}) async-start(), calls=%async_computation.1 | async-start | bytes 1179648 | tf_op jit(solution)/shard_map/all_gather | solution.py:54
  7.9 86.4 %all-gather.9.cloned.1.call-start = ((), (), s32[]{:S(2)}) async-start(), calls=%async_computation.2 | async-start | bytes 1179648 | tf_op jit(solution)/shard_map/all_gather | solution.py:55
  8.7 126.8 %all-gather.11.cloned.1.call-start = ((), (), s32[]{:S(2)}) async-start(), calls=%async_computation.3 | async-start | bytes 1179648 | tf_op jit(solution)/shard_map/all_gather | solution.py:56
  9.4 6.0 %copy-start.6 = (bf16[2048,256]{1,0:T(8,128)(2,1)S(1)}, bf16[2048,256]{1,0:T(8,128)(2,1)}, u32[]{:S(2)}) copy-start(bf16[2048,256]{1,0:T(8,128)(2,1)} %param.17) | copy-start | bytes 3145732
  9.4 193.5 %reduce-scatter.4.cloned.1.call-start = ((), (), s32[]{:S(2)}) async-start(), calls=%async_computation.7 | async-start | bytes 884736
  9.5 11.9 %slice-start = ((s8[8388608]{0:T(1024)(128)(4,1)}), s8[4194304]{0:T(1024)(128)(4,1)S(1)}, s32[]{:S(2)}) async-start(s8[8388608]{0:T(1024)(128)(4,1)} %bitcast.42), calls=%async_computation.8 | async-start | bytes 8388608
  15.4 5.9 %slice-start.1 = ((s8[8388608]{0:T(1024)(128)(4,1)}), s8[4194304]{0:T(1024)(128)(4,1)S(1)}, s32[]{:S(2)}) async-start(s8[8388608]{0:T(1024)(128)(4,1)} %bitcast.42), calls=%async_computation.9 | async-start | bytes 8388608
  15.4 5.9 %copy-start.7 = (bf16[2048,256]{1,0:T(8,128)(2,1)S(1)}, bf16[2048,256]{1,0:T(8,128)(2,1)}, u32[]{:S(2)}) copy-start(bf16[2048,256]{1,0:T(8,128)(2,1)} %param.15) | copy-start | bytes 3145732
  53.2 43.2 %copy-start.8 = (bf16[2048,256]{1,0:T(8,128)(2,1)S(1)}, bf16[2048,256]{1,0:T(8,128)(2,1)}, u32[]{:S(2)}) copy-start(bf16[2048,256]{1,0:T(8,128)(2,1)} %all-gather.7.cloned.1.call-done) | copy-start | bytes 3145732
  94.3 3.8 copy-start.9
  137.4 3.4 copy-start.3
  137.5 3.4 copy-start.4
  137.5 3.4 copy-start.5
  139.5 65.1 %copy-start.2 = (f32[256,256]{1,0:T(8,128)S(1)}, f32[256,256]{1,0:T(8,128)}, u32[]{:S(2)}) copy-start(f32[256,256]{1,0:T(8,128)} %param.21) | copy-start | bytes 786436
  140.8 178.0 %all-gather.17.cloned.1.call-start = ((), (), s32[]{:S(2)}) async-start(), calls=%async_computation.6 | async-start | bytes 1179648 | tf_op jit(solution)/shard_map/all_gather | solution.py:81
  278.0 8.7 %copy-start.1 = (f32[256,256]{1,0:T(8,128)}, f32[256,256]{1,0:T(8,128)S(1)}, u32[]{:S(2)}) copy-start(f32[256,256]{1,0:T(8,128)S(1)} %fusion.14) | copy-start | bytes 786436
  278.9 80.5 %all-gather.15.cloned.1.call-start = ((), (), s32[]{:S(2)}) async-start(), calls=%async_computation.5 | async-start | bytes 1179648 | tf_op jit(solution)/shard_map/all_gather | solution.py:80
  281.8 118.6 %all-gather.13.cloned.1.call-start = ((), (), s32[]{:S(2)}) async-start(), calls=%async_computation.4 | async-start | bytes 1179648 | tf_op jit(solution)/shard_map/all_gather | solution.py:79
Sparse Core Ops, SparseCore 0:
  10.1 42.9 all-gather.6
  55.3 38.9 all-gather.8
  96.4 38.9 all-gather.10
  140.9 61.9 reduce-scatter.3
  279.0 39.7 all-gather.16
  321.2 38.0 all-gather.14
  362.0 38.3 all-gather.12
where the time goes:
time: 410 us
  waiting for transfers between devices  272 us (66%)
  blocking collectives  71.1 us (17%)
  matrix products  30.3 us (7%)
  between operations  15.2 us (4%)
  local copies, waits for them, and re-layouts  13.9 us (3%)
  other arithmetic  6.34 us (2%)
    unnamed x8, waiting for transfers between devices  63.8 us
    psum x1, blocking collectives, body(): total = lax.psum(jnp.sum(projected * projected), ('fs', 'tp'))  40.2 us
    all_gather x1, waiting for transfers between devices, body(): lax.all_gather(p_value, 'fs', axis=0, tiled=True)  39.1 us
    all_gather x1, waiting for transfers between devices, body(): lax.all_gather(fresh_key, 'fs', axis=0, tiled=True)  38.8 us
    all_gather x1, waiting for transfers between devices, body(): lax.all_gather(fresh_value, 'fs', axis=0, tiled=True)  38.4 us
    all_gather x1, waiting for transfers between devices, body(): lax.all_gather(p_out, 'fs', axis=0, tiled=True)  35.7 us
    all_gather x1, waiting for transfers between devices, body(): lax.all_gather(fresh_out, 'fs', axis=1, tiled=True)  31.3 us
    all_gather x1, blocking collectives, body(): gathered = lax.all_gather(direction, 'fs', axis=0, tiled=True)  31 us
  transfers between devices with their start and end apart: 7, of which 7 were waited for; matrix products, arithmetic and copies ran while one was open for 10% of the time, Pallas kernels for 0%

commit v1 on v0

v1 whole, which is shorter than its diff:
```python
import functools

import jax
import jax.numpy as jnp
from jax import lax
from jax.experimental import pallas as pl
from jax.experimental.pallas import tpu as pltpu
from jax.sharding import PartitionSpec as P

beta_one = 0.9
beta_two = 0.9
learn_rate = 0.01
MESH = pl.DeviceIdType.MESH
f32 = jnp.float32
bf16 = jnp.bfloat16


def remote(src, dst, send_sem, recv_sem, target):
    return pltpu.make_async_remote_copy(
        src_ref=src, dst_ref=dst, send_sem=send_sem, recv_sem=recv_sem,
        device_id=target, device_id_type=MESH,
    )


class Gather:
    def __init__(self, view, send_sem, recv, place, span, order, sibling=None):
        self.view, self.send_sem, self.recv = view, send_sem, recv
        self.z, self.b = place
        self.span, self.order, self.sibling = span, order, sibling
        self.sends = []

    def index(self, z, b):
        return z * 2 + b

    def send(self, cond, z, b, to):
        j = self.index(z, b)

        def copy():
            return remote(self.view(j), self.view(j), self.send_sem, self.recv.at[j], {"fs": to})

        if cond is None:
            copy().start()
        else:
            pl.when(cond)(lambda: copy().start())
        self.sends.append((cond, copy))

    def to_sibling(self, cond, z, b):
        if self.sibling is None:
            return
        target, recv = self.sibling
        j = self.index(z, b)

        def copy():
            return remote(self.view(j), self.view(j), self.send_sem, recv.at[j], {"tp": target})

        if cond is None:
            copy().start()
        else:
            pl.when(cond)(lambda: copy().start())
        self.sends.append((cond, copy))

    def arrive(self, cond, z, b):
        j = self.index(z, b)

        def wait():
            remote(self.view(j), self.view(j), self.send_sem, self.recv.at[j], {"fs": j}).wait_recv()

        if cond is None:
            wait()
        else:
            pl.when(cond)(wait)

    def up_down(self, b):
        z = self.z
        self.send(z < self.span - 1, z, b, self.index(z + 1, self.b))
        self.send(z > 0, z, b, self.index(z - 1, self.b))

    def begin(self):
        z, b = self.z, self.b
        pair = self.index(z, 1 - b)
        if self.order == "line":
            self.up_down(b)
            self.send(None, z, b, pair)
        else:
            self.send(None, z, b, pair)
            self.up_down(b)
        self.to_sibling(None, z, b)

    def cross(self):
        if self.order == "pair":
            self.arrive(None, self.z, 1 - self.b)
            self.up_down(1 - self.b)
            self.to_sibling(None, self.z, 1 - self.b)

    def step(self, s):
        z, b, span = self.z, self.b, self.span
        for b_from in (b,) if self.order == "line" else (b, 1 - b):
            for sign in (1, -1):
                zf = z - sign * s
                have = (zf >= 0) if sign == 1 else (zf < span)
                more = (z < span - 1) if sign == 1 else (z > 0)
                self.arrive(have, zf, b_from)
                self.send(jnp.logical_and(have, more), zf, b_from, self.index(z + sign, b))
                if self.order == "line":
                    self.send(have, zf, b, self.index(z, 1 - b))
                self.to_sibling(have, zf, b_from)

    def cross_end(self):
        if self.order == "line":
            for zf in range(self.span):
                self.arrive(None, zf, 1 - self.b)
                self.to_sibling(None, zf, 1 - self.b)

    def sibling_end(self, view):
        target, recv = self.sibling
        for j in range(2 * self.span):
            remote(view(j), view(j), self.send_sem, recv.at[j], {"tp": target}).wait_recv()

    def finish(self):
        for cond, copy in self.sends:
            if cond is None:
                copy().wait_send()
            else:
                pl.when(cond)(lambda copy=copy: copy().wait_send())


def kernel(
    n, t, chunk, entries,
    x_hbm, y_hbm, k_hbm, v_hbm, h_hbm, p_in, w_in, mk_in, mv_in, mo_in,
    p_out, w_out, d_out, nk_out, nv_out, no_out,
    x_buf, y_buf, c_buf, ct_buf, g_buf, part_out, part_in, sq_tp, sq_fs, sq_sum,
    load_sem, own_sem, g_send, pa_recv, pb_recv, pa_sib, pb_sib, wa_recv, wb_recv,
    r_send, r_recv, st_send, st_recv, sf_send, sf_recv, d_send, d_recv,
):
    me, tp = lax.axis_index("fs"), lax.axis_index("tp")
    place = (me // 2, me % 2)
    span = n // 2
    half = tp % 2
    sibling = tp + 1 - 2 * half
    tokens, width = x_hbm.shape
    columns = k_hbm.shape[1]
    rows = part_in.shape[1]
    n_chunks = width // chunk

    loads = [
        pltpu.make_async_copy(src, c_buf.at[:, pl.ds(i * columns, columns)], load_sem.at[i])
        for i, src in enumerate((k_hbm, v_hbm, h_hbm))
    ]
    x_loads = [
        pltpu.make_async_copy(src.at[:, pl.ds(c * chunk, chunk)], dst.at[c], load_sem.at[3 + o * n_chunks + c])
        for o, (src, dst) in enumerate(((x_hbm, x_buf), (y_hbm, y_buf)))
        for c in range(n_chunks)
    ]
    own_p = pltpu.make_async_copy(p_in, p_out.at[:, pl.ds(2 * me, 2)], own_sem.at[0])
    own_w = pltpu.make_async_copy(w_in, w_out.at[:, me], own_sem.at[1])
    own_p.start()
    own_w.start()
    for load in loads + x_loads:
        load.start()

    barrier = pltpu.get_barrier_semaphore()
    for k in range(1, n):
        pl.semaphore_signal(barrier, inc=1, device_id={"fs": lax.rem(me + k, n)}, device_id_type=MESH)
    for k in range(1, t):
        pl.semaphore_signal(barrier, inc=1, device_id={"tp": lax.rem(tp + k, t)}, device_id_type=MESH)
    pl.semaphore_wait(barrier, n + t - 2)

    def p_view(low, high, side):
        return lambda j: p_out.at[low:high, 2 * j + side]

    own_p.wait()
    own_w.wait()
    pa = Gather(p_view(0, 2, half), g_send.at[0], pa_recv, place, span, "line", (sibling, pa_sib))
    pb = Gather(p_view(2, 3, half), g_send.at[1], pb_recv, place, span, "pair", (sibling, pb_sib))
    wa = Gather(lambda j: w_out.at[0:2, j], g_send.at[2], wa_recv, place, span, "line")
    wb = Gather(lambda j: w_out.at[2:3, j], g_send.at[3], wb_recv, place, span, "pair")
    sib_a, pa.sibling = pa.sibling, None
    sib_b, pb.sibling = pb.sibling, None
    pb.begin()
    pa.begin()
    pa.sibling, pb.sibling = sib_a, sib_b

    for load in loads:
        load.wait()
    ct_buf[...] = c_buf[...].T

    def grads(o, c):
        x_loads[o * n_chunks + c].wait()
        lo, hi = (0, 2 * columns) if o == 0 else (2 * columns, 3 * columns)
        g_buf[lo:hi, c * chunk:(c + 1) * chunk] = jnp.dot(
            ct_buf[lo:hi, :], (x_buf, y_buf)[o][c], preferred_element_type=f32
        ).astype(bf16)

    work = [(o, c) for o in range(2) for c in range(n_chunks)]
    per = -(-len(work) // (span - 1 + 1))
    todo = list(work)

    def some():
        for _ in range(per):
            if todo:
                grads(*todo.pop(0))

    some()
    pb.cross()
    for s in range(1, span):
        pa.step(s)
        pb.step(s)
        some()
    while todo:
        grads(*todo.pop(0))
    pa.cross_end()
    wb.begin()
    wa.begin()

    def sib_end(gather, low, high):
        target, recv = gather.sibling
        view = p_view(low, high, 1 - half)
        for j in range(n):
            @pl.when(me != j)
            def _():
                remote(view(j), view(j), gather.send_sem, recv.at[j], {"tp": target}).wait_recv()

    sib_end(pa, 0, 2)
    sib_end(pb, 2, 3)

    for m in range(3):
        full = p_out[m].reshape(width, p_out.shape[3])
        proj = jnp.dot(g_buf[m * columns:(m + 1) * columns, :], full, preferred_element_type=f32)
        part_out[:, :, m * columns:(m + 1) * columns] = proj.T.astype(bf16).reshape(n, rows, columns)

    part_copies = []
    for k in range(1, n):
        to = lax.rem(me + k, n)
        copy = remote(part_out.at[to], part_in.at[k], r_send.at[k], r_recv.at[k], {"fs": to})
        copy.start()
        part_copies.append(copy)
    wb.cross()
    total = part_out[me].astype(f32)
    for copy in part_copies:
        copy.wait_recv()
    for k in range(1, n):
        total = total + part_in[k].astype(f32)

    squares = jnp.sum(total * total, axis=0, keepdims=True)
    square = jnp.sum(squares, axis=1, keepdims=True)
    sq_tp[tp] = jnp.broadcast_to(square, (8, 128))
    tp_copies = []
    for k in range(1, t):
        to = lax.rem(tp + k, t)
        copy = remote(sq_tp.at[tp], sq_tp.at[tp], st_send.at[k], st_recv.at[k], {"tp": to})
        copy.start()
        tp_copies.append(copy)
    for copy in tp_copies:
        copy.wait_recv()
    sum_tp = sq_tp[0]
    for k in range(1, t):
        sum_tp = sum_tp + sq_tp[k]
    sq_fs[me] = sum_tp
    fs_copies = []
    for k in range(1, n):
        to = lax.rem(me + k, n)
        copy = remote(sq_fs.at[me], sq_fs.at[me], sf_send.at[k], sf_recv.at[k], {"fs": to})
        copy.start()
        fs_copies.append(copy)
    for copy in fs_copies:
        copy.wait_recv()
    sum_fs = sq_fs[0]
    for k in range(1, n):
        sum_fs = sum_fs + sq_fs[k]
    scale = 1.0 / jnp.sqrt(sum_fs[0:1, 0:1] / entries + 1e-06)
    normed = total * scale

    for m, (old, new) in enumerate(((mk_in, nk_out), (mv_in, nv_out), (mo_in, no_out))):
        q = normed[:, m * columns:(m + 1) * columns]
        one = beta_one * old[0] + (1 - beta_one) * q
        two = beta_two * old[1] + (1 - beta_two) * q * q
        new[0] = one
        new[1] = two
        d_out[me, :, m * columns:(m + 1) * columns] = (one / jnp.sqrt(two)).astype(bf16)
    d_copies = []
    for k in range(1, n):
        to = lax.rem(me + k, n)
        copy = remote(d_out.at[me], d_out.at[me], d_send.at[k], d_recv.at[k], {"fs": to})
        copy.start()
        d_copies.append(copy)
    for s in range(1, span):
        wa.step(s)
        wb.step(s)
    wa.cross_end()
    for copy in d_copies:
        copy.wait_recv()
    for copy in part_copies + tp_copies + fs_copies + d_copies:
        copy.wait_send()
    for gather in (pa, pb, wa, wb):
        gather.finish()


def body(
    x_saved, h_saved, key_cot, value_cot, out_cot, w_key, w_value, w_out,
    p_key, p_value, p_out, m_key, m_value, m_out,
):
    n, t = lax.axis_size("fs"), lax.axis_size("tp")
    tokens, width = x_saved.shape
    columns = key_cot.shape[1]
    local, rank = p_key.shape
    rows = rank // n
    chunk = min(512, width)
    n_chunks = width // chunk
    p_stack = jnp.stack([p_key, p_value, p_out]).reshape(3, 2, local // 2, rank)
    w_stack = jnp.stack([w_key.astype(bf16), w_value.astype(bf16), w_out.T.astype(bf16)])
    entries = 3 * rank * columns * t
    any_spec = pl.BlockSpec(memory_space=pl.ANY)
    vmem = pl.BlockSpec(memory_space=pltpu.VMEM)
    dma = pltpu.SemaphoreType.DMA
    moment = jax.ShapeDtypeStruct(m_key.shape, f32)
    p_full, w_full, d_full, new_k, new_v, new_o = pl.pallas_call(
        functools.partial(kernel, n, t, chunk, entries),
        out_shape=(
            jax.ShapeDtypeStruct((3, 2 * n, local // 2, rank), bf16),
            jax.ShapeDtypeStruct((3, n, local, columns), bf16),
            jax.ShapeDtypeStruct((n, rows, 3 * columns), bf16),
            moment, moment, moment,
        ),
        in_specs=[any_spec] * 5 + [vmem] * 5,
        out_specs=(vmem,) * 6,
        scratch_shapes=[
            pltpu.VMEM((n_chunks, tokens, chunk), bf16),
            pltpu.VMEM((n_chunks, tokens, chunk), bf16),
            pltpu.VMEM((tokens, 3 * columns), bf16),
            pltpu.VMEM((3 * columns, tokens), bf16),
            pltpu.VMEM((3 * columns, width), bf16),
            pltpu.VMEM((n, rows, 3 * columns), bf16),
            pltpu.VMEM((n, rows, 3 * columns), bf16),
            pltpu.VMEM((t, 8, 128), f32),
            pltpu.VMEM((n, 8, 128), f32),
            pltpu.VMEM((8, 128), f32),
            dma((3 + 2 * n_chunks,)),
            dma((2,)),
            dma((4,)),
            dma((n,)), dma((n,)), dma((n,)), dma((n,)), dma((n,)), dma((n,)),
            dma((n,)), dma((n,)), dma((t,)), dma((t,)),
            dma((n,)), dma((n,)), dma((n,)), dma((n,)),
        ],
        compiler_params=pltpu.CompilerParams(
            collective_id=0, has_side_effects=True, vmem_limit_bytes=60 * 1024 * 1024
        ),
        name="fused_update",
    )(x_saved, out_cot, key_cot, value_cot, h_saved, p_stack, w_stack, m_key, m_value, m_out)

    direction = d_full.reshape(rank, 3 * columns)
    factors = p_full.reshape(3, width, rank)
    weights = w_full.reshape(3, width, columns)
    parts = [direction[:, m * columns:(m + 1) * columns] for m in range(3)]
    dot = functools.partial(jnp.dot, preferred_element_type=f32)
    step_key, step_value = dot(p_key, parts[0]), dot(p_value, parts[1])
    step_out = dot(parts[2].T, p_out.T)
    copies = [
        (weights[m].astype(f32) - learn_rate * dot(factors[m], parts[m])).astype(bf16)
        for m in range(2)
    ]
    copy_out = (weights[2].T.astype(f32) - learn_rate * dot(parts[2].T, factors[2].T)).astype(bf16)
    return (step_key, step_value, step_out, copies[0], copies[1], copy_out, new_k, new_v, new_o)


def solution(mesh):
    in_specs = (
        P("fs", None), P("fs", "tp"), P("fs", "tp"), P("fs", "tp"), P("fs", None),
        P("fs", "tp"), P("fs", "tp"), P("tp", "fs"),
        P("fs", None), P("fs", None), P("fs", None),
        P(None, "fs", "tp"), P(None, "fs", "tp"), P(None, "fs", "tp"),
    )
    out_specs = (
        P("fs", "tp"), P("fs", "tp"), P("tp", "fs"),
        P(None, "tp"), P(None, "tp"), P("tp", None),
        P(None, "fs", "tp"), P(None, "fs", "tp"), P(None, "fs", "tp"),
    )
    return jax.shard_map(body, mesh=mesh, in_specs=in_specs, out_specs=out_specs, check_vma=False)
```

time: 410 us -> 110 us (0.27)
  waiting for transfers between devices: 272 us -> 0 us
  Pallas kernels: 0 us -> 86.8 us
  blocking collectives: 71.1 us -> 0 us
  matrix products: 30.3 us -> 7.51 us
  between operations: 15.2 us -> 0.76 us
  local copies, waits for them, and re-layouts: 13.9 us -> 9.69 us
    all_gather x6 -> x0, waiting for transfers between devices: 209 us -> none  [the longest x1 39.1 us: body(): lax.all_gather(p_value, 'fs', axis=0, tiled=True)]
    pallas_call x0 -> x1, Pallas kernels: none -> 86.8 us  [body(): pl.pallas_call(functools.partial(kernel, n, t, chunk, entries), out_shape...]
    unnamed x8 -> x0, waiting for transfers between devices: 63.8 us -> none
    psum x1 -> x0, blocking collectives: 40.2 us -> none  [body(): total = lax.psum(jnp.sum(projected * projected), ('fs', 'tp'))]
    all_gather x1 -> x0, blocking collectives: 31 us -> none  [body(): gathered = lax.all_gather(direction, 'fs', axis=0, tiled=True)]
    dot_general x12 -> x6, matrix products: 30.3 us -> 7.51 us  [the longest x2 2.82 us: body(): dot(factors[m], parts[m])]
    unnamed x38 -> x22, local copies, waits for them, and re-layouts: 13.4 us -> 5.17 us
  transfers between devices with their start and end apart: 7 -> 0, of which waited for: 7 -> 0; matrix products, arithmetic and copies ran while one was open for 10% -> 0% of each run, Pallas kernels for 0% -> 0%
where the time goes in v1:
time: 110 us
  Pallas kernels  86.8 us (79%)
  local copies, waits for them, and re-layouts  9.69 us (9%)
  matrix products  7.51 us (7%)
  other arithmetic  5.23 us (5%)
    pallas_call x1, Pallas kernels, body(): pl.pallas_call(functools.partial(kernel, n, t, chunk, entries), out_shape...  86.8 us
    unnamed x22, local copies, waits for them, and re-layouts  5.17 us
    dot_general x2, matrix products, body(): dot(factors[m], parts[m])  2.82 us
    slice x1, local copies, waits for them, and re-layouts, body(): factors[2]  2.3 us
    dot_general x2, matrix products, body(): step_key, step_value = (dot(p_key, parts[0]), dot(p_value, parts[1]))  2.3 us

profile of v1, /device:TPU:0, one launch (start us, length us, event | category | flops | bytes accessed | tf_op | source)
XLA Modules:
  0.0 110.0 jit_solution(10821896927965919838)
XLA Ops:
  0.6 1.8 %pad_maximum_fusion.p_in = bf16[3,2,128,256]{3,2,1,0:T(8,128)(2,1)} fusion(bf16[1,2,128,256]{3,2,1,0:T(8,128)(2,1)} %bitcast.49, bf16[1,2,128,256]{3,2,1,0:T(8,128)(2,1)} %bitcast.48, bf16[1,2,128,256]{3,2,1,0:T(8,128)(2,1)} %bitcast.47), kind=kLoop, calls=%fused_computation.12 | loop fusion | flops 393216 | bytes 786432 | tf_op jit(solution)/shard_map/stack | solution.py:309
  2.5 1.0 copy.23
  3.5 1.1 convert_bitcast_fusion.1
  4.6 0.8 pad_maximum_fusion.1.w_in
  5.4 0.0 copy-start.2
  5.4 0.0 copy-start.3
  5.4 86.8 %fused_update.1 = (bf16[3,16,128,256]{3,2,1,0:T(8,128)(2,1)}, bf16[3,8,256,256]{3,2,1,0:T(8,128)(2,1)}, bf16[8,32,768]{2,1,0:T(8,128)(2,1)}, f32[2,32,256]{2,1,0...) custom-call(bf16[2048,2048]{1,0:T(8,128)(2,1)} %x_hbm.1, bf16[2048,2048]{1,0:T(8,128)(2,1)} %y_hbm.1, ...), custom_call_target="tpu_custom_call" | custom-call | tf_op jit(solution)/shard_map/fused_update/pallas_call | solution.py:316
  92.2 0.0 copy-start.1
  92.2 0.0 copy-start.4
  92.2 0.0 copy-done.2
  92.2 1.2 %convolution_bitcast_fusion.1 = f32[256,256]{0,1:T(8,128)S(1)} fusion(bf16[256,256]{1,0:T(8,128)(2,1)S(1)} %copy-done.2, bf16[256,768]{1,0:T(8,128)(2,1)} %bitcast.40), kind=kOutput, calls=%fused_computation.10 | convolution fusion | flops 33554432 | bytes 524288 | tf_op jit(solution)/shard_map/dot_general | solution.py:355
  93.4 0.8 copy.25
  94.2 0.0 copy-done.3
  94.2 1.1 %convolution_bitcast_fusion = f32[256,256]{0,1:T(8,128)S(1)} fusion(bf16[256,256]{1,0:T(8,128)(2,1)S(1)} %copy-done.3, bf16[256,768]{1,0:T(8,128)(2,1)} %bitcast.41), kind=kOutput, calls=%fused_computation.9 | convolution fusion | flops 33554432 | bytes 524288 | tf_op jit(solution)/shard_map/dot_general | solution.py:355
  95.3 0.8 copy.26
  96.2 0.0 copy-done.1
  96.2 0.0 copy-done.4
  96.2 0.9 fusion.7
  97.1 0.0 copy-start
  97.1 2.3 %fusion.14 = (bf16[1,16,128,256]{3,2,1,0:T(8,128)(2,1)S(1)}, bf16[1,16,128,256]{3,2,1,0:T(8,128)(2,1)S(1)}, bf16[1,16,128,256]{3,2,1,0:T(8,128)(2,1)S(1)}) fusion(bf16[3,16,128,256]{3,2,1,0:T(8,128)(2,1)} %get-tuple-element.17), kind=kLoop, calls=%fused_computation.25 | loop fusion | bytes 6291456 | tf_op jit(solution)/shard_map/slice | solution.py:361
  99.4 0.5 copy-done
  100.0 0.3 fusion.13
  100.3 1.4 %fusion.3 = bf16[2048,256]{1,0:T(8,128)(2,1)} fusion(bf16[2048,256]{1,0:T(8,128)(2,1)S(1)} %bitcast.36, bf16[2048,256]{1,0:T(8,128)(2,1)S(1)} %bitcast.38, bf16[256,768]{1,0:T(8,128)(2,1)S(1)} %bitcast.43), kind=kOutput, calls=%fused_computation.6 | convolution fusion | flops 270532608 | bytes 3276800 | tf_op jit(solution)/shard_map/dot_general | solution.py:358
  101.7 1.4 %fusion.4 = bf16[2048,256]{1,0:T(8,128)(2,1)} fusion(bf16[2048,256]{1,0:T(8,128)(2,1)S(1)} %bitcast.35, bf16[2048,256]{1,0:T(8,128)(2,1)S(1)} %bitcast.37, bf16[256,768]{1,0:T(8,128)(2,1)S(1)} %bitcast.44), kind=kOutput, calls=%fused_computation.7 | convolution fusion | flops 270532608 | bytes 3276800 | tf_op jit(solution)/shard_map/dot_general | solution.py:358
  103.1 1.6 %bitcast_convert_fusion = f32[2048,256]{1,0:T(8,128)} fusion(bf16[1,8,256,256]{3,2,1,0:T(8,128)(2,1)S(1)} %get-tuple-element.30), kind=kLoop, calls=%fused_computation.11 | loop fusion | flops 524288 | bytes 3145728 | tf_op jit(solution)/shard_map/convert_element_type | solution.py:361
  104.6 1.9 %copy.24 = f32[2048,256]{0,1:T(8,128)S(1)} copy(f32[2048,256]{1,0:T(8,128)} %bitcast_convert_fusion) | data formatting | bytes 4194304 | tf_op jit(solution)/shard_map/convert_element_type | solution.py:361
  106.6 0.0 copy-start.7
  106.6 0.0 copy-start.6
  106.6 0.0 copy-start.5
  106.6 1.5 %fusion.5 = bf16[256,2048]{1,0:T(8,128)(2,1)} fusion(bf16[2048,256]{1,0:T(8,128)(2,1)S(1)} %bitcast.39, f32[2048,256]{0,1:T(8,128)S(1)} %copy.24, bf16[256,768]{1,0:T(8,128)(2,1)S(1)} %bitcast.45), kind=kOutput, calls=%fused_computation.8 | convolution fusion | flops 270008320 | bytes 4325376 | tf_op jit(solution)/shard_map/dot_general | solution.py:361
  108.1 0.0 copy-done.7
  108.1 0.6 copy.30
  108.7 0.0 copy-done.6
  108.7 0.6 copy.31
  109.3 0.0 copy-done.5
  109.3 0.6 copy.32
Async XLA Ops:
  5.4 86.8 %copy-start.2 = (bf16[256,256]{1,0:T(8,128)(2,1)S(1)}, bf16[256,256]{1,0:T(8,128)(2,1)}, u32[]{:S(2)}) copy-start(bf16[256,256]{1,0:T(8,128)(2,1)} %param.22) | copy-start | bytes 393220
  5.4 88.8 %copy-start.3 = (bf16[256,256]{1,0:T(8,128)(2,1)S(1)}, bf16[256,256]{1,0:T(8,128)(2,1)}, u32[]{:S(2)}) copy-start(bf16[256,256]{1,0:T(8,128)(2,1)} %param.23) | copy-start | bytes 393220
  92.2 4.0 %copy-start.1 = (bf16[8,32,768]{2,1,0:T(8,128)(2,1)S(1)}, bf16[8,32,768]{2,1,0:T(8,128)(2,1)}, u32[]{:S(2)}) copy-start(bf16[8,32,768]{2,1,0:T(8,128)(2,1)} %get-tuple-element.15) | copy-start | bytes 1179652
  92.2 4.0 %copy-start.4 = (bf16[256,256]{1,0:T(8,128)(2,1)S(1)}, bf16[256,256]{1,0:T(8,128)(2,1)}, u32[]{:S(2)}) copy-start(bf16[256,256]{1,0:T(8,128)(2,1)} %param.24) | copy-start | bytes 393220
  97.1 2.8 %copy-start = (bf16[3,8,256,256]{3,2,1,0:T(8,128)(2,1)S(1)}, bf16[3,8,256,256]{3,2,1,0:T(8,128)(2,1)}, u32[]{:S(2)}) copy-start(bf16[3,8,256,256]{3,2,1,0:T(8,128)(2,1)} %get-tuple-element.16) | copy-start | bytes 9437188
  106.6 1.5 %copy-start.7 = (f32[2,32,256]{2,1,0:T(8,128)S(1)}, f32[2,32,256]{2,1,0:T(8,128)}, u32[]{:S(2)}) copy-start(f32[2,32,256]{2,1,0:T(8,128)} %get-tuple-element.53) | copy-start | bytes 196612
  106.6 2.1 %copy-start.6 = (f32[2,32,256]{2,1,0:T(8,128)S(1)}, f32[2,32,256]{2,1,0:T(8,128)}, u32[]{:S(2)}) copy-start(f32[2,32,256]{2,1,0:T(8,128)} %get-tuple-element.54) | copy-start | bytes 196612
  106.6 2.7 %copy-start.5 = (f32[2,32,256]{2,1,0:T(8,128)S(1)}, f32[2,32,256]{2,1,0:T(8,128)}, u32[]{:S(2)}) copy-start(f32[2,32,256]{2,1,0:T(8,128)} %get-tuple-element.55) | copy-start | bytes 196612

commit v2 on v1

--- a/solution.py
+++ b/solution.py
@@ -124,12 +124,42 @@
                 pl.when(cond)(lambda copy=copy: copy().wait_send())
 
 
+def moments(old, q):
+    return (
+        beta_one * old[0] + (1 - beta_one) * q,
+        beta_two * old[1] + (1 - beta_two) * q * q,
+    )
+
+
+def finish_kernel(
+    columns, p_ref, w_ref, d_ref, q_ref, pk_ref, pv_ref, po_ref, mk_ref, mv_ref, mo_ref,
+    sk_ref, sv_ref, so_ref, ck_ref, cv_ref, co_ref, nk_ref, nv_ref, no_ref,
+):
+    def step(factor, m):
+        return jnp.dot(factor, d_ref[:, m * columns:(m + 1) * columns], preferred_element_type=f32)
+
+    def fresh(m):
+        return (w_ref[m].astype(f32) - learn_rate * step(p_ref[m], m)).astype(bf16)
+
+    ck_ref[...] = fresh(0)
+    cv_ref[...] = fresh(1)
+    co_ref[...] = fresh(2).T
+
+    @pl.when(pl.program_id(0) == 0)
+    def _():
+        sk_ref[...] = step(pk_ref[...], 0)
+        sv_ref[...] = step(pv_ref[...], 1)
+        so_ref[...] = step(po_ref[...], 2).T
+        for m, (old, new) in enumerate(((mk_ref, nk_ref), (mv_ref, nv_ref), (mo_ref, no_ref))):
+            new[0], new[1] = moments(old, q_ref[:, m * columns:(m + 1) * columns])
+
+
 def kernel(
     n, t, chunk, entries,
-    x_hbm, y_hbm, k_hbm, v_hbm, h_hbm, p_in, w_in, mk_in, mv_in, mo_in,
-    p_out, w_out, d_out, nk_out, nv_out, no_out,
-    x_buf, y_buf, c_buf, ct_buf, g_buf, part_out, part_in, sq_tp, sq_fs, sq_sum,
-    load_sem, own_sem, g_send, pa_recv, pb_recv, pa_sib, pb_sib, wa_recv, wb_recv,
+    x_hbm, y_hbm, k_hbm, v_hbm, h_hbm, pk_hbm, pv_hbm, po_hbm, wk_hbm, wv_hbm, wo_hbm, mk_in, mv_in, mo_in,
+    p_out, w_out, d_out, q_out,
+    x_buf, y_buf, c_buf, ct_buf, g_buf, wk_buf, wv_buf, wo_buf, part_out, part_in, sq_tp, sq_fs,
+    load_sem, own_sem, g_send, p_recv, p_sib, w_recv,
     r_send, r_recv, st_send, st_recv, sf_send, sf_recv, d_send, d_recv,
 ):
     me, tp = lax.axis_index("fs"), lax.axis_index("tp")
@@ -151,11 +181,17 @@
         for o, (src, dst) in enumerate(((x_hbm, x_buf), (y_hbm, y_buf)))
         for c in range(n_chunks)
     ]
-    own_p = pltpu.make_async_copy(p_in, p_out.at[:, pl.ds(2 * me, 2)], own_sem.at[0])
-    own_w = pltpu.make_async_copy(w_in, w_out.at[:, me], own_sem.at[1])
-    own_p.start()
-    own_w.start()
-    for load in loads + x_loads:
+    own_p = [
+        pltpu.make_async_copy(src, p_out.at[m, pl.ds(2 * me, 2)], own_sem.at[m])
+        for m, src in enumerate((pk_hbm, pv_hbm, po_hbm))
+    ]
+    own_w = [
+        pltpu.make_async_copy(src, dst, own_sem.at[3 + m])
+        for m, (src, dst) in enumerate(((wk_hbm, wk_buf), (wv_hbm, wv_buf), (wo_hbm, wo_buf)))
+    ]
+    for load in own_p:
+        load.start()
+    for load in loads + x_loads + own_w:
         load.start()
 
     barrier = pltpu.get_barrier_semaphore()
@@ -165,20 +201,24 @@
         pl.semaphore_signal(barrier, inc=1, device_id={"tp": lax.rem(tp + k, t)}, device_id_type=MESH)
     pl.semaphore_wait(barrier, n + t - 2)
 
-    def p_view(low, high, side):
-        return lambda j: p_out.at[low:high, 2 * j + side]
-
-    own_p.wait()
-    own_w.wait()
-    pa = Gather(p_view(0, 2, half), g_send.at[0], pa_recv, place, span, "line", (sibling, pa_sib))
-    pb = Gather(p_view(2, 3, half), g_send.at[1], pb_recv, place, span, "pair", (sibling, pb_sib))
-    wa = Gather(lambda j: w_out.at[0:2, j], g_send.at[2], wa_recv, place, span, "line")
-    wb = Gather(lambda j: w_out.at[2:3, j], g_send.at[3], wb_recv, place, span, "pair")
-    sib_a, pa.sibling = pa.sibling, None
-    sib_b, pb.sibling = pb.sibling, None
-    pb.begin()
-    pa.begin()
-    pa.sibling, pb.sibling = sib_a, sib_b
+    def p_view(m, side):
+        return lambda j: p_out.at[m, 2 * j + side]
+
+    def w_view(m):
+        return lambda j: w_out.at[m, j]
+
+    for load in own_p:
+        load.wait()
+    orders = ("line", "line", "pair")
+    ps = [
+        Gather(p_view(m, half), g_send.at[m], p_recv.at[m], place, span, orders[m], (sibling, p_sib.at[m]))
+        for m in range(3)
+    ]
+    ws = [Gather(w_view(m), g_send.at[3 + m], w_recv.at[m], place, span, orders[m]) for m in range(3)]
+    for m in (2, 0, 1):
+        to, ps[m].sibling = ps[m].sibling, None
+        ps[m].begin()
+        ps[m].sibling = to
 
     for load in loads:
         load.wait()
@@ -201,27 +241,30 @@
                 grads(*todo.pop(0))
 
     some()
-    pb.cross()
+    ps[2].cross()
     for s in range(1, span):
-        pa.step(s)
-        pb.step(s)
+        for m in (0, 1, 2):
+            ps[m].step(s)
+        if s == 1:
+            for load in own_w:
+                load.wait()
+            w_out[0, me] = wk_buf[...].astype(bf16)
+            w_out[1, me] = wv_buf[...].astype(bf16)
+            w_out[2, me] = wo_buf[...].T.astype(bf16)
         some()
     while todo:
         grads(*todo.pop(0))
-    pa.cross_end()
-    wb.begin()
-    wa.begin()
-
-    def sib_end(gather, low, high):
-        target, recv = gather.sibling
-        view = p_view(low, high, 1 - half)
+    for m in (2, 0, 1):
+        ws[m].begin()
+    for m in (0, 1):
+        ps[m].cross_end()
+    for m in range(3):
+        target, recv = ps[m].sibling
+        view = p_view(m, 1 - half)
         for j in range(n):
             @pl.when(me != j)
-            def _():
-                remote(view(j), view(j), gather.send_sem, recv.at[j], {"tp": target}).wait_recv()
-
-    sib_end(pa, 0, 2)
-    sib_end(pb, 2, 3)
+            def _(view=view, recv=recv, m=m, target=target, j=j):
+                remote(view(j), view(j), ps[m].send_sem, recv.at[j], {"tp": target}).wait_recv()
 
     for m in range(3):
         full = p_out[m].reshape(width, p_out.shape[3])
@@ -234,7 +277,10 @@
         copy = remote(part_out.at[to], part_in.at[k], r_send.at[k], r_recv.at[k], {"fs": to})
         copy.start()
         part_copies.append(copy)
-    wb.cross()
+    ws[2].cross()
+    for s in range(1, min(2, span)):
+        for m in (0, 1, 2):
+            ws[m].step(s)
     total = part_out[me].astype(f32)
     for copy in part_copies:
         copy.wait_recv()
@@ -262,6 +308,9 @@
         copy = remote(sq_fs.at[me], sq_fs.at[me], sf_send.at[k], sf_recv.at[k], {"fs": to})
         copy.start()
         fs_copies.append(copy)
+    for s in range(2, min(3, span)):
+        for m in (0, 1):
+            ws[m].step(s)
     for copy in fs_copies:
         copy.wait_recv()
     sum_fs = sq_fs[0]
@@ -270,12 +319,9 @@
     scale = 1.0 / jnp.sqrt(sum_fs[0:1, 0:1] / entries + 1e-06)
     normed = total * scale
 
-    for m, (old, new) in enumerate(((mk_in, nk_out), (mv_in, nv_out), (mo_in, no_out))):
-        q = normed[:, m * columns:(m + 1) * columns]
-        one = beta_one * old[0] + (1 - beta_one) * q
-        two = beta_two * old[1] + (1 - beta_two) * q * q
-        new[0] = one
-        new[1] = two
+    q_out[...] = normed
+    for m, old in enumerate((mk_in, mv_in, mo_in)):
+        one, two = moments(old, normed[:, m * columns:(m + 1) * columns])
         d_out[me, :, m * columns:(m + 1) * columns] = (one / jnp.sqrt(two)).astype(bf16)
     d_copies = []
     for k in range(1, n):
@@ -283,15 +329,19 @@
         copy = remote(d_out.at[me], d_out.at[me], d_send.at[k], d_recv.at[k], {"fs": to})
         copy.start()
         d_copies.append(copy)
-    for s in range(1, span):
-        wa.step(s)
-        wb.step(s)
-    wa.cross_end()
+    for s in range(2, min(3, span)):
+        for m in (2,):
+            ws[m].step(s)
+    for s in range(3, span):
+        for m in (0, 1, 2):
+            ws[m].step(s)
+    for m in (0, 1):
+        ws[m].cross_end()
     for copy in d_copies:
         copy.wait_recv()
     for copy in part_copies + tp_copies + fs_copies + d_copies:
         copy.wait_send()
-    for gather in (pa, pb, wa, wb):
+    for gather in ps + ws:
         gather.finish()
 
 
@@ -306,38 +356,39 @@
     rows = rank // n
     chunk = min(512, width)
     n_chunks = width // chunk
-    p_stack = jnp.stack([p_key, p_value, p_out]).reshape(3, 2, local // 2, rank)
-    w_stack = jnp.stack([w_key.astype(bf16), w_value.astype(bf16), w_out.T.astype(bf16)])
+    halves = [p.reshape(2, local // 2, rank) for p in (p_key, p_value, p_out)]
     entries = 3 * rank * columns * t
     any_spec = pl.BlockSpec(memory_space=pl.ANY)
     vmem = pl.BlockSpec(memory_space=pltpu.VMEM)
     dma = pltpu.SemaphoreType.DMA
-    moment = jax.ShapeDtypeStruct(m_key.shape, f32)
-    p_full, w_full, d_full, new_k, new_v, new_o = pl.pallas_call(
+    shape = jax.ShapeDtypeStruct
+    p_full, w_full, d_full, normed = pl.pallas_call(
         functools.partial(kernel, n, t, chunk, entries),
         out_shape=(
-            jax.ShapeDtypeStruct((3, 2 * n, local // 2, rank), bf16),
-            jax.ShapeDtypeStruct((3, n, local, columns), bf16),
-            jax.ShapeDtypeStruct((n, rows, 3 * columns), bf16),
-            moment, moment, moment,
+            shape((3, 2 * n, local // 2, rank), bf16),
+            shape((3, n, local, columns), bf16),
+            shape((n, rows, 3 * columns), bf16),
+            shape((rows, 3 * columns), f32),
         ),
-        in_specs=[any_spec] * 5 + [vmem] * 5,
-        out_specs=(vmem,) * 6,
+        in_specs=[any_spec] * 11 + [vmem] * 3,
+        out_specs=(vmem,) * 4,
         scratch_shapes=[
             pltpu.VMEM((n_chunks, tokens, chunk), bf16),
             pltpu.VMEM((n_chunks, tokens, chunk), bf16),
             pltpu.VMEM((tokens, 3 * columns), bf16),
             pltpu.VMEM((3 * columns, tokens), bf16),
             pltpu.VMEM((3 * columns, width), bf16),
+            pltpu.VMEM((local, columns), f32),
+            pltpu.VMEM((local, columns), f32),
+            pltpu.VMEM((columns, local), f32),
             pltpu.VMEM((n, rows, 3 * columns), bf16),
             pltpu.VMEM((n, rows, 3 * columns), bf16),
             pltpu.VMEM((t, 8, 128), f32),
             pltpu.VMEM((n, 8, 128), f32),
-            pltpu.VMEM((8, 128), f32),
             dma((3 + 2 * n_chunks,)),
-            dma((2,)),
-            dma((4,)),
-            dma((n,)), dma((n,)), dma((n,)), dma((n,)), dma((n,)), dma((n,)),
+            dma((6,)),
+            dma((6,)),
+            dma((3, n)), dma((3, n)), dma((3, n)),
             dma((n,)), dma((n,)), dma((t,)), dma((t,)),
             dma((n,)), dma((n,)), dma((n,)), dma((n,)),
         ],
@@ -345,21 +396,43 @@
             collective_id=0, has_side_effects=True, vmem_limit_bytes=60 * 1024 * 1024
         ),
         name="fused_update",
-    )(x_saved, out_cot, key_cot, value_cot, h_saved, p_stack, w_stack, m_key, m_value, m_out)
-
-    direction = d_full.reshape(rank, 3 * columns)
-    factors = p_full.reshape(3, width, rank)
-    weights = w_full.reshape(3, width, columns)
-    parts = [direction[:, m * columns:(m + 1) * columns] for m in range(3)]
-    dot = functools.partial(jnp.dot, preferred_element_type=f32)
-    step_key, step_value = dot(p_key, parts[0]), dot(p_value, parts[1])
-    step_out = dot(parts[2].T, p_out.T)
-    copies = [
-        (weights[m].astype(f32) - learn_rate * dot(factors[m], parts[m])).astype(bf16)
-        for m in range(2)
-    ]
-    copy_out = (weights[2].T.astype(f32) - learn_rate * dot(parts[2].T, factors[2].T)).astype(bf16)
-    return (step_key, step_value, step_out, copies[0], copies[1], copy_out, new_k, new_v, new_o)
+    )(
+        x_saved, out_cot, key_cot, value_cot, h_saved, *halves,
+        w_key, w_value, w_out, m_key, m_value, m_out,
+    )
+
+    block = min(512, width)
+    whole = lambda *dims: pl.BlockSpec(dims, lambda i: (0,) * len(dims))
+    moment = whole(*m_key.shape)
+    factor = whole(local, rank)
+    return pl.pallas_call(
+        functools.partial(finish_kernel, columns),
+        grid=(width // block,),
+        out_shape=(
+            shape((local, columns), f32), shape((local, columns), f32), shape((columns, local), f32),
+            shape((width, columns), bf16), shape((width, columns), bf16), shape((columns, width), bf16),
+            shape(m_key.shape, f32), shape(m_key.shape, f32), shape(m_key.shape, f32),
+        ),
+        in_specs=[
+            pl.BlockSpec((3, block, rank), lambda i: (0, i, 0)),
+            pl.BlockSpec((3, block, columns), lambda i: (0, i, 0)),
+            whole(rank, 3 * columns), whole(rows, 3 * columns),
+            factor, factor, factor, moment, moment, moment,
+        ],
+        out_specs=(
+            whole(local, columns), whole(local, columns), whole(columns, local),
+            pl.BlockSpec((block, columns), lambda i: (i, 0)),
+            pl.BlockSpec((block, columns), lambda i: (i, 0)),
+            pl.BlockSpec((columns, block), lambda i: (0, i)),
+            moment, moment, moment,
+        ),
+        compiler_params=pltpu.CompilerParams(dimension_semantics=("arbitrary",)),
+        name="finish",
+    )(
+        p_full.reshape(3, width, rank), w_full.reshape(3, width, columns),
+        d_full.reshape(rank, 3 * columns), normed,
+        p_key, p_value, p_out, m_key, m_value, m_out,
+    )
 
 
 def solution(mesh):

time: 110 us -> 84.5 us (0.77)
  local copies, waits for them, and re-layouts: 9.69 us -> 0 us
  matrix products: 7.51 us -> 0 us
  other arithmetic: 5.23 us -> 0 us
  Pallas kernels: 86.8 us -> 83.6 us
    pallas_call x1, Pallas kernels: 86.8 us -> 77 us  [body(): pl.pallas_call(functools.partial(kernel, n, t, chunk, entries), out_shape...]
    dot_general x6 -> x0, matrix products: 7.51 us -> none  [the longest x2 2.82 us: body(): dot(factors[m], parts[m])]
    pallas_call x0 -> x1, Pallas kernels: none -> 6.58 us  [body(): pl.pallas_call(functools.partial(finish_kernel, columns), grid=(width //...]
    unnamed x22 -> x0, local copies, waits for them, and re-layouts: 5.17 us -> none
    another operation x3 -> x0, other arithmetic: 3.67 us -> none  [the longest x2 1.85 us: body(): jnp.stack([w_key.astype(bf16), w_value.astype(bf16), w_out.T.astype(bf16)])]
    slice x2 -> x0, local copies, waits for them, and re-layouts: 2.6 us -> none  [the longest x1 2.3 us: body(): factors[2]]
    convert_element_type x1 -> x0, local copies, waits for them, and re-layouts: 1.92 us -> none  [body(): weights[2].T.astype(f32) - learn_rate * dot(parts[2].T, factors[2].T)]
    convert_element_type x1 -> x0, other arithmetic: 1.56 us -> none  [body(): weights[2].T.astype(f32) - learn_rate * dot(parts[2].T, factors[2].T)]
where the time goes in v2:
time: 84.5 us; the launch traced here: 84.3 us
  Pallas kernels  83.6 us (99%)
    pallas_call x1, Pallas kernels, body(): pl.pallas_call(functools.partial(kernel, n, t, chunk, entries), out_shape...  77 us
    pallas_call x1, Pallas kernels, body(): pl.pallas_call(functools.partial(finish_kernel, columns), grid=(width //...  6.58 us

profile of v2, /device:TPU:0, one launch (start us, length us, event | category | flops | bytes accessed | tf_op | source)
XLA Modules:
  0.0 84.3 jit_solution(5141985848140964024)
XLA Ops:
  0.6 77.0 %fused_update.1 = (bf16[3,16,128,256]{3,2,1,0:T(8,128)(2,1)}, bf16[3,8,256,256]{3,2,1,0:T(8,128)(2,1)}, bf16[8,32,768]{2,1,0:T(8,128)(2,1)}, f32[32,768]{1,0:T(8,128)}) custom-call(bf16[2048,2048]{1,0:T(8,128)(2,1)} %x_hbm.1, bf16[2048,2048]{1,0:T(8,128)(2,1)} %y_hbm.1, bf16[2048,256]{1,0:T(8,128)(2,1)} %k_hbm.1, bf16[2048,256]{1,0:T(8,128)(2,1)} %v_hbm.1, ...), custom_call_target="tpu_custom_call" | custom-call | tf_op jit(solution)/shard_map/fused_update/pallas_call | solution.py:365
  77.7 6.6 %finish.1 = (f32[256,256]{1,0:T(8,128)}, f32[256,256]{1,0:T(8,128)}, f32[256,256]{1,0:T(8,128)}, bf16[2048,256]{1,0:T(8,128)(2,1)}, bf16[2048,256]{1,0:T(8,128)(...) custom-call(bf16[3,2048,256]{2,1,0:T(8,128)(2,1)} %bitcast.6, ...), custom_call_target="tpu_custom_call" | custom-call | tf_op jit(solution)/shard_map/finish/pallas_call | solution.py:408
